TPU v7x, 512 devices: a whole 4x8x8 slice. The times are simulated.
512 devices in a mesh: rep: 2 (over z_hi), fs: 32 (over z_lo, y), tp: 8 (over x, core).
Axes of the slice: x: 4, y: 8, z: 8 (z_hi: 2, z_lo: 4; z = z_hi * 4 + z_lo), core: 2. Of those that a mesh axis runs over, the one named last changes fastest.
Arguments:
- tokens: bfloat16 [32768, 2048], P(('rep', 'fs'), 'tp'), may hold values from -6 to 6
- mix_gain: float32 [2048], replicated, may hold values from 0.1 to 1.9
- query_w: bfloat16 [2048, 2048], P('fs', 'tp'), may hold values from -0.125 to 0.125
- key_w: bfloat16 [2048, 2048], P('fs', 'tp'), may hold values from -0.125 to 0.125
- value_w: bfloat16 [2048, 4096], P('fs', 'tp'), may hold values from -0.125 to 0.125
- head_gain: float32 [8, 512], replicated, may hold values from 0.1 to 1.9
- out_w: bfloat16 [4096, 2048], P('tp', 'fs'), may hold values from -0.09375 to 0.09375
- chan_gain: float32 [2048], replicated, may hold values from 0.1 to 1.9
- up_w: bfloat16 [2048, 4096], P('fs', 'tp'), may hold values from -0.125 to 0.125
- down_w: bfloat16 [4096, 2048], P('tp', 'fs'), may hold values from -0.09375 to 0.09375
Outputs:
- layer_out: bfloat16 [32768, 2048], P(('rep', 'fs'), 'tp')
All inputs are finite; a program needn't handle non-finite values.
Results may differ from a plain program's by a relative error of at most 0.019.
Values may be sent and summed in bfloat16 or wider, within the bound.
A program may use at most 64 MiB of HBM per device.

v0:
```python
import jax
import jax.numpy as jnp
from jax import lax
from jax.sharding import PartitionSpec as P

DK = 256
DV = 512
BLOCK = 128


EPS = 1e-06
HEAD_EPS = 0.05
THETA = 10000.0


def gather_turned(arrays, axis, dims):
    turned = [jnp.moveaxis(a, dim, 0) for a, dim in zip(arrays, dims)]
    both = jnp.concatenate([t.reshape(len(t), -1) for t in turned], axis=1)
    whole, at, finished = (lax.all_gather(both, axis, axis=0, tiled=True), 0, [])
    for t, dim in zip(turned, dims):
        section = whole[:, at : at + t[0].size].reshape(-1, *t.shape[1:])
        finished.append(jnp.moveaxis(section, 0, dim))
        at += t[0].size
    return tuple(finished)


def in_order(blocks, dim):
    shape = list(blocks.shape[1:])
    shape[dim] *= blocks.shape[0]
    return jnp.moveaxis(blocks, 0, dim).reshape(shape)


def copy_for_each(value, axis):
    count = lax.axis_size(axis)
    return lax.all_to_all(
        jnp.broadcast_to(value[None], (count, *value.shape)), axis, 0, 0, tiled=True
    )


def gathered_copies(value, axis, dim):
    return in_order(copy_for_each(value, axis), dim)


def cut_along(value, dim, count):
    shape = value.shape
    blocks = value.reshape(*shape[:dim], count, shape[dim] // count, *shape[dim + 1 :])
    return jnp.moveaxis(blocks, dim, 0)


def sum_at_owner(value, axis, dim):
    count = lax.axis_size(axis)
    blocks = lax.all_to_all(cut_along(value, dim, count), axis, 0, 0, tiled=True)
    return jnp.sum(blocks.astype(jnp.float32), axis=0)


def norm_rows(rows, gain):
    values = rows.astype(jnp.float32)
    scale = lax.rsqrt(jnp.mean(values * values, axis=-1, keepdims=True) + EPS)
    return (values * scale * gain).astype(jnp.bfloat16)


def rotate(field, places):
    half = field.shape[-1] // 2
    inverse = THETA ** (-jnp.arange(half, dtype=jnp.float32) / half)
    angles = places[:, None] * inverse
    cosine = jnp.cos(angles)[:, None, :]
    sine = jnp.sin(angles)[:, None, :]
    first = field[..., :half]
    second = field[..., half:]
    return jnp.concatenate(
        [first * cosine - second * sine, second * cosine + first * sine], axis=-1
    )


def retain(query, keys, values, log_rate):
    count = query.shape[0] // BLOCK
    q_blocks = query.reshape(count, BLOCK, query.shape[1])
    k_blocks = keys.reshape(count, BLOCK, keys.shape[1])
    v_blocks = values.reshape(count, BLOCK, values.shape[1])
    place = jnp.arange(BLOCK, dtype=jnp.float32)
    offset = place[:, None] - place[None, :]
    mask = jnp.where(offset >= 0, jnp.exp(log_rate * jnp.maximum(offset, 0.0)), 0.0)
    q_decay = jnp.exp(log_rate * (place + 1.0))
    k_decay = jnp.exp(log_rate * (BLOCK - 1.0 - place))
    block_decay = jnp.exp(log_rate * BLOCK)

    def advance(state, item):
        q_part, k_part, v_part = item
        scores = jnp.dot(q_part, k_part.T, preferred_element_type=jnp.float32)
        weights = (scores * mask).astype(jnp.bfloat16)
        result = jnp.dot(weights, v_part, preferred_element_type=jnp.float32)
        q_scaled = (q_part.astype(jnp.float32) * q_decay[:, None]).astype(jnp.bfloat16)
        result = result + jnp.dot(
            q_scaled, state.astype(jnp.bfloat16), preferred_element_type=jnp.float32
        )
        k_scaled = (k_part.astype(jnp.float32) * k_decay[:, None]).astype(jnp.bfloat16)
        state = state * block_decay + jnp.dot(
            k_scaled.T, v_part, preferred_element_type=jnp.float32
        )
        return (state, result)

    start = jnp.zeros((query.shape[1], values.shape[1]), jnp.float32)
    _, outputs = lax.scan(advance, start, (q_blocks, k_blocks, v_blocks))
    return outputs.reshape(count * BLOCK, values.shape[1])


def shards(tokens, mix_gain, query_w, key_w, value_w, head_gain, out_w, chan_gain, up_w, down_w):
    rows = tokens.shape[0]
    local = query_w.shape[1] // DK
    query_all, key_all, value_all, out_all, up_all, down_all = gather_turned(
        (query_w, key_w, value_w, out_w, up_w, down_w), "fs", (0, 0, 0, 1, 0, 1)
    )
    whole = gathered_copies(tokens, "tp", 1)
    normed = norm_rows(whole, mix_gain)
    qraw = jnp.dot(normed, query_all, preferred_element_type=jnp.float32)
    kraw = jnp.dot(normed, key_all, preferred_element_type=jnp.float32)
    vraw = jnp.dot(normed, value_all, preferred_element_type=jnp.float32)
    places = jnp.arange(rows, dtype=jnp.int32).astype(jnp.float32)
    query = rotate(qraw.reshape(rows, local, DK), places).astype(jnp.bfloat16)
    keys = (rotate(kraw.reshape(rows, local, DK), places) * DK ** (-0.5)).astype(jnp.bfloat16)
    values = vraw.reshape(rows, local, DV).astype(jnp.bfloat16)
    first_head = lax.axis_index("tp") * local
    heads = (first_head + jnp.arange(local, dtype=jnp.int32)).astype(jnp.float32)
    log_rate = jnp.log1p(-jnp.exp2(-5.0 - heads))
    retained = jax.vmap(retain, in_axes=(1, 1, 1, 0), out_axes=1)(query, keys, values, log_rate)
    gains = lax.dynamic_slice_in_dim(head_gain, first_head, local, 0)
    scale = lax.rsqrt(jnp.mean(retained * retained, axis=-1, keepdims=True) + HEAD_EPS)
    head_out = (retained * scale * gains).astype(jnp.bfloat16).reshape(rows, local * DV)
    mixer_terms = jnp.dot(head_out, out_all, preferred_element_type=jnp.float32)
    mixed = sum_at_owner(mixer_terms.astype(jnp.bfloat16), "tp", 1)
    middle = (tokens.astype(jnp.float32) + mixed).astype(jnp.bfloat16)
    whole_middle = gathered_copies(middle, "tp", 1)
    chan_normed = norm_rows(whole_middle, chan_gain)
    upward = jnp.dot(chan_normed, up_all, preferred_element_type=jnp.float32)
    hidden = jnp.square(jax.nn.relu(upward)).astype(jnp.bfloat16)
    chan_terms = jnp.dot(hidden, down_all, preferred_element_type=jnp.float32)
    channel = sum_at_owner(chan_terms.astype(jnp.bfloat16), "tp", 1)
    return (middle.astype(jnp.float32) + channel).astype(jnp.bfloat16)


def solution(mesh):
    placed = (
        P(("rep", "fs"), "tp"),
        P(),
        P("fs", "tp"),
        P("fs", "tp"),
        P("fs", "tp"),
        P(),
        P("tp", "fs"),
        P(),
        P("fs", "tp"),
        P("tp", "fs"),
    )
    return jax.shard_map(
        shards, mesh=mesh, in_specs=placed, out_specs=P(("rep", "fs"), "tp"), check_vma=False
    )
```

profile of v0, /device:TPU:1, one launch (start us, length us, event | category | flops | bytes accessed | tf_op | source)
XLA Modules:
  0.0 313.0 jit_solution(4496840921103430434)
XLA Ops:
  6.5 0.8 constant_dynamic-update-slice_fusion.3
  7.3 0.8 constant_dynamic-update-slice_fusion.2
  8.1 0.8 constant_dynamic-update-slice_fusion.1
  8.9 0.8 bitcast_dynamic-update-slice_fusion.1
  9.8 0.8 constant_dynamic-update-slice_fusion
  10.6 0.8 bitcast_dynamic-update-slice_fusion
  11.5 0.7 copy-done.5
  12.2 1.1 copy.23
  13.3 1.5 broadcast_in_dim.15
  14.8 10.3 %all-to-all-start = ((bf16[8,512,256]{1,2,0:T(8,128)(2,1)}), bf16[8,512,256]{1,2,0:T(8,128)(2,1)S(1)}, u32[]{:S(2)}, u32[]{:S(2)}) async-start(bf16[8,512,256]{1,2,0:T(8,128)(2,1)} %broadcast_in_dim.15), calls=%async_computation | async-start | bytes 4194304 | tf_op jit(solution)/shard_map/all_to_all | solution.py:35
  25.3 26.1 %all-to-all-done = bf16[8,512,256]{1,2,0:T(8,128)(2,1)S(1)} async-done(((bf16[8,512,256]{1,2,0:T(8,128)(2,1)}), bf16[8,512,256]{1,2,0:T(8,128)(2,1)S(1)}, u32[]{:S(2)}, u32[]{:S(2)}) %all-to-all-start) | async-done | bytes 2097184 | tf_op jit(solution)/shard_map/all_to_all | solution.py:35
  51.5 0.5 multiply_reduce_fusion.1
  52.0 1.9 fusion.57
  53.8 117.0 %all-gather.2.cloned.1.call-done = bf16[2048,2560]{1,0:T(8,128)(2,1)} async-done(((bf16[64,2560]{1,0:T(8,128)(2,1)}), bf16[2048,2560]{1,0:T(8,128)(2,1)}) %all-gather.2.cloned.1.call-update) | async-done | bytes 10485776 | tf_op jit(solution)/shard_map/all_gather | solution.py:19
  170.9 2.6 convolution_bitcast_fusion.2
  173.5 2.0 convolution_bitcast_fusion.1
  175.5 1.2 fusion.95
  177.0 3.0 fusion.70
  180.0 3.8 %while.15 = (s32[]{:T(128)}, f32[1,256,512]{2,1,0:T(8,128)S(1)}, f32[4,1,128,512]{3,2,1,0:T(8,128)S(1)}, f32[1]{0:T(128)}, bf16[4,1,128,256]{3,2,1,0:T(8,128)(2,...) while((s32[]{:T(128)}, f32[1,256,512]{2,1,0:T(8,128)S(1)}, ...), condition=%wide.region_2.3_spmd.clone.clone.clone, body=%wide.region_1.2_spmd.clone.clone.clone.sunk | while | flops 93176320 | bytes 2890356 | solution.py:103
  180.0 0.3 fusion.122
  181.0 0.3 fusion.122
  181.9 0.3 fusion.122
  182.9 0.3 fusion.122
  184.2 2.9 convolution_convert_fusion.1
  187.2 49.3 %all_to_all.20 = bf16[8,512,256]{2,1,0:T(8,128)(2,1)S(1)} all-to-all(bf16[8,512,256]{2,1,0:T(8,128)(2,1)S(1)} %bitcast.148), channel_id=1, replica_groups=mesh['rep'=2,'fs'=32,'tp'=8] {'tp'}, dimensions={0} | all-to-all | bytes 4194304 | tf_op jit(solution)/shard_map/all_to_all | solution.py:52
  236.8 0.6 copy-done.4
  237.8 29.7 %all_to_all.21 = bf16[8,512,256]{1,2,0:T(8,128)(2,1)S(1)} all-to-all(bf16[8,512,256]{1,2,0:T(8,128)(2,1)S(1)} %broadcast_in_dim.16), channel_id=1, replica_groups=mesh['rep'=2,'fs'=32,'tp'=8] {'tp'}, dimensions={0} | all-to-all | bytes 4194304 | tf_op jit(solution)/shard_map/all_to_all | solution.py:35
  267.5 0.5 multiply_reduce_fusion
  268.2 1.9 fusion.55
  270.0 5.2 %convolution_convert_fusion = bf16[512,2048]{1,0:T(8,128)(2,1)S(1)} fusion(bf16[2048,2560]{1,0:T(8,128)(2,1)} %all-gather.2.cloned.1.call-done, bf16[512,2048]{0,1:T(8,128)(2,1)} %fusion.55), kind=kOutput, calls=%fused_computation.61 | convolution fusion | flops 2149318656 | bytes 8388608 | tf_op jit(solution)/shard_map/dot_general | solution.py:136
  275.4 29.7 %all_to_all.22 = bf16[8,512,256]{2,1,0:T(8,128)(2,1)S(1)} all-to-all(bf16[8,512,256]{2,1,0:T(8,128)(2,1)S(1)} %bitcast.149), channel_id=1, replica_groups=mesh['rep'=2,'fs'=32,'tp'=8] {'tp'}, dimensions={0} | all-to-all | bytes 4194304 | tf_op jit(solution)/shard_map/all_to_all | solution.py:52
  305.4 0.8 add_convert_fusion
  (47 shorter events, 4.4 us)
Async XLA Ops:
  6.5 18.7 %copy-start = (f32[8,512]{1,0:T(8,128)S(1)}, f32[8,512]{1,0:T(8,128)}, u32[]{:S(2)}) copy-start(f32[8,512]{1,0:T(8,128)} %param.17) | copy-start | bytes 49156
  6.5 164.3 %all-gather.2.cloned.1.call-start = ((), (), s32[]{:S(2)}) async-start(), calls=%async_computation.4 | async-start | bytes 10813440 | tf_op jit(solution)/shard_map/all_gather | solution.py:19
  11.4 0.7 copy-start.5
  14.8 36.7 %all-to-all-start = ((bf16[8,512,256]{1,2,0:T(8,128)(2,1)}), bf16[8,512,256]{1,2,0:T(8,128)(2,1)S(1)}, u32[]{:S(2)}, u32[]{:S(2)}) async-start(bf16[8,512,256]{1,2,0:T(8,128)(2,1)} %broadcast_in_dim.15), calls=%async_computation | async-start | bytes 4194304 | tf_op jit(solution)/shard_map/all_to_all | solution.py:35
  25.1 26.9 %copy-start.6 = (f32[2048]{0:T(1024)S(1)}, f32[2048]{0:T(1024)}, u32[]{:S(2)}) copy-start(f32[2048]{0:T(1024)} %param.13) | copy-start | bytes 24580
  53.8 119.6 %copy-start.2 = (bf16[512,2048]{0,1:T(8,128)(2,1)S(1)}, bf16[512,2048]{0,1:T(8,128)(2,1)}, u32[]{:S(2)}) copy-start(bf16[512,2048]{0,1:T(8,128)(2,1)} %fusion.57) | copy-start | bytes 6291460
  175.5 1.6 copy-start.3
  177.0 3.0 copy-start.1
  236.5 1.0 copy-start.4
  267.5 0.7 copy-start.7
Sparse Core Ops, SparseCore 0:
  12.3 158.5 all-gather.1
where the time goes:
time: 314 us; the launch traced here: 313 us
  waiting for transfers between devices  143 us (46%)
  blocking collectives  109 us (35%)
  matrix products  19.2 us (6%)
  between operations  13.7 us (4%)
  starting transfers between devices  10.3 us (3%)
  local copies, waits for them, and re-layouts  9.88 us (3%)
  other arithmetic  7.86 us (3%)
    all_gather x1, waiting for transfers between devices, gather_turned(): lax.all_gather(both, axis, axis=0, tiled=True)  117 us
    all_to_all x2, blocking collectives, sum_at_owner(): lax.all_to_all(cut_along(value, dim, count), axis, 0, 0, tiled=True)  78.9 us
    all_to_all x1, blocking collectives, copy_for_each(): lax.all_to_all(jnp.broadcast_to(value[None], (count, *value.shape)), axis...  29.7 us
    all_to_all x1, waiting for transfers between devices, copy_for_each(): lax.all_to_all(jnp.broadcast_to(value[None], (count, *value.shape)), axis...  26.1 us
    all_to_all x1, starting transfers between devices, copy_for_each(): lax.all_to_all(jnp.broadcast_to(value[None], (count, *value.shape)), axis...  10.3 us
    unnamed x22, local copies, waits for them, and re-layouts  6.96 us
  transfers between devices with their start and end apart: 2, of which 2 were waited for; matrix products, arithmetic and copies ran while one was open for 2% of the time, Pallas kernels for 0%

commit v1 on v0

--- a/solution.py
+++ b/solution.py
@@ -1,6 +1,11 @@
+import functools
+import heapq
+
 import jax
 import jax.numpy as jnp
 from jax import lax
+from jax.experimental import pallas as pl
+from jax.experimental.pallas import tpu as pltpu
 from jax.sharding import PartitionSpec as P
 
 DK = 256
@@ -13,15 +18,148 @@
 THETA = 10000.0
 
 
-def gather_turned(arrays, axis, dims):
-    turned = [jnp.moveaxis(a, dim, 0) for a, dim in zip(arrays, dims)]
-    both = jnp.concatenate([t.reshape(len(t), -1) for t in turned], axis=1)
-    whole, at, finished = (lax.all_gather(both, axis, axis=0, tiled=True), 0, [])
-    for t, dim in zip(turned, dims):
-        section = whole[:, at : at + t[0].size].reshape(-1, *t.shape[1:])
-        finished.append(jnp.moveaxis(section, 0, dim))
-        at += t[0].size
-    return tuple(finished)
+def neighbours(route, a, b, unit):
+    out = []
+    two = lambda k: 1 if k % 2 == 0 else -1
+    if route == "A":
+        fw = 4 if unit % 4 < 2 else 3
+        bw = 7 - fw
+        if b == 0:
+            if 0 <= a < fw: out.append(("y", 1))
+            if 0 >= a > -bw: out.append(("y", -1))
+            out += [("z", 1), ("z", -1)]
+        elif abs(b) == 1 and two(a) == b:
+            out.append(("z", b))
+    else:
+        fw = 4 if b % 2 == 0 else 3
+        bw = 7 - fw
+        if a == 0:
+            if b == 0: out += [("z", 1), ("z", -1)]
+            elif abs(b) == 1 and two(unit // 2) == b: out.append(("z", b))
+        if 0 <= a < fw: out.append(("y", 1))
+        if 0 >= a > -bw: out.append(("y", -1))
+    return out
+
+def simulate(routes, group, service=1.45, latency=1.8, lead=3.2, start=None):
+    start = start or [0.0] * len(routes)
+    def down(u, a, b):
+        n = neighbours(routes[u], a, b, u)
+        return max([0] + [1 + down(u, a + (s if ax == "y" else 0), b + (s if ax == "z" else 0)) for ax, s in n])
+    free = {(ax, s): 0.0 for ax in "yz" for s in (1, -1)}
+    pending = {k: [] for k in free}
+    events = []
+    actions = []
+    seq = 0
+    arrivals = [(start[u], 0, u, 0, 0) for u in range(len(routes))]
+    heapq.heapify(arrivals)
+    index = {}
+    counts = [0] * len(routes)
+    now = 0.0
+    arrived = {}
+    while arrivals or any(pending.values()):
+        t_link = min([max(free[k], min(p[2] for p in pending[k])) for k in free if pending[k]], default=float("inf"))
+        t_arr = arrivals[0][0] if arrivals else float("inf")
+        if t_arr <= t_link:
+            t, hop, u, a, b = heapq.heappop(arrivals)
+            arrived[(u, a, b)] = t
+            if (a, b) != (0, 0):
+                index[(u, a, b)] = counts[u]; counts[u] += 1
+                actions.append((t, 0, ("wait", u, a, b)))
+            for ax, s in neighbours(routes[u], a, b, u):
+                na, nb = a + (s if ax == "y" else 0), b + (s if ax == "z" else 0)
+                pending[(ax, s)].append((group[u], -(1 + down(u, na, nb)), t, u, a, b, na, nb))
+        else:
+            k = min((k for k in free if pending[k]), key=lambda k: max(free[k], min(p[2] for p in pending[k])))
+            t0 = t_link
+            ready = [p for p in pending[k] if p[2] <= t0 + 1e-9]
+            p = min(ready)
+            pending[k].remove(p)
+            free[k] = t0 + service
+            g, d, t, u, a, b, na, nb = p
+            actions.append((max(t, t0 - lead), 1, ("send", u, a, b, na, nb, k)))
+            heapq.heappush(arrivals, (t0 + service + latency, 1, u, na, nb))
+    actions.sort(key=lambda x: (x[0], x[1]))
+    return actions, index, counts, arrived
+
+
+ROUTES = "ABABA"
+GROUPS = (0, 0, 1, 2, 2)
+NY, NZ = 8, 4
+MESH = pl.DeviceIdType.MESH
+
+
+def gather_kernel(*refs):
+    parts, units = refs[:5], refs[5:10]
+    local_sem, send_sem, recv_sem = refs[10:]
+    rep, fs = lax.axis_index("rep"), lax.axis_index("fs")
+    z, y = fs // NY, fs % NY
+    z_up, z_down = (z + 1) % NZ, (z + NZ - 1) % NZ
+    away = {
+        ("y", 1): (rep, z * NY + (y + 1) % NY),
+        ("y", -1): (rep, z * NY + (y + NY - 1) % NY),
+        ("z", 1): ((rep + (z + 1) // NZ) % 2, z_up * NY + y),
+        ("z", -1): ((rep + (NZ - z) // NZ) % 2, z_down * NY + y),
+    }
+    target = {k: {"rep": r, "fs": f} for k, (r, f) in away.items()}
+
+    def slot(a, b):
+        at = ((z - b + NZ) % NZ) * NY + (y - a + NY) % NY
+        return pl.ds(pl.multiple_of(at * 64, 64), 64)
+
+    barrier = pltpu.get_barrier_semaphore()
+    for k in target:
+        pl.semaphore_signal(barrier, inc=1, device_id=target[k], device_id_type=MESH)
+    local = []
+    for u in range(5):
+        copy = pltpu.make_async_copy(parts[u], units[u].at[slot(0, 0)], local_sem.at[u])
+        copy.start()
+        local.append(copy)
+    for copy in local:
+        copy.wait()
+    pl.semaphore_wait(barrier, 4)
+
+    actions, index, counts, _ = simulate(ROUTES, GROUPS)
+
+    def copy_of(n, u, a, b, na, nb, k):
+        return pltpu.make_async_remote_copy(
+            src_ref=units[u].at[slot(a, b)],
+            dst_ref=units[u].at[slot(a, b)],
+            send_sem=send_sem.at[n],
+            recv_sem=recv_sem.at[u, index[u, na, nb]],
+            device_id=target[k],
+            device_id_type=MESH,
+        )
+
+    sends = []
+    for _, _, action in actions:
+        if action[0] == "wait":
+            _, u, a, b = action
+            here = units[u].at[slot(a, b)]
+            pltpu.make_async_copy(here, here, recv_sem.at[u, index[u, a, b]]).wait()
+        else:
+            copy = copy_of(len(sends), *action[1:])
+            copy.start()
+            sends.append(copy)
+    for copy in sends:
+        copy.wait_send()
+
+
+def gather_units(parts):
+    return pl.pallas_call(
+        gather_kernel,
+        out_shape=[jax.ShapeDtypeStruct((2048, 512), jnp.bfloat16)] * 5,
+        in_specs=[pl.BlockSpec(memory_space=pl.ANY)] * 5,
+        out_specs=[pl.BlockSpec(memory_space=pltpu.VMEM)] * 5,
+        scratch_shapes=[
+            pltpu.SemaphoreType.DMA((5,)),
+            pltpu.SemaphoreType.DMA((155,)),
+            pltpu.SemaphoreType.DMA((5, 31)),
+        ],
+        compiler_params=pltpu.CompilerParams(
+            collective_id=0, has_side_effects=True, vmem_limit_bytes=60 << 20
+        ),
+        name="gather_units",
+    )(*parts)
 
 
 def in_order(blocks, dim):
@@ -107,9 +245,10 @@
 def shards(tokens, mix_gain, query_w, key_w, value_w, head_gain, out_w, chan_gain, up_w, down_w):
     rows = tokens.shape[0]
     local = query_w.shape[1] // DK
-    query_all, key_all, value_all, out_all, up_all, down_all = gather_turned(
-        (query_w, key_w, value_w, out_w, up_w, down_w), "fs", (0, 0, 0, 1, 0, 1)
-    )
+    parts = (jnp.concatenate([query_w, key_w], axis=1), value_w, out_w.T, up_w, down_w.T)
+    both, value_all, out_turned, up_all, down_turned = gather_units(parts)
+    query_all, key_all = both[:, :DK], both[:, DK:]
+    out_all, down_all = out_turned.T, down_turned.T
     whole = gathered_copies(tokens, "tp", 1)
     normed = norm_rows(whole, mix_gain)
     qraw = jnp.dot(normed, query_all, preferred_element_type=jnp.float32)

time: 314 us -> 203 us (0.65)
  waiting for transfers between devices: 143 us -> 0.01 us
  Pallas kernels: 0 us -> 69.4 us
  blocking collectives: 109 us -> 94.9 us
  between operations: 13.7 us -> 0.39 us
  matrix products: 19.2 us -> 12.8 us
    all_gather x1 -> x0, waiting for transfers between devices: 117 us -> none  [gather_turned(): lax.all_gather(both, axis, axis=0, tiled=True)]
    pallas_call x0 -> x1, Pallas kernels: none -> 69.4 us  [gather_units(): pl.pallas_call(gather_kernel, out_shape=[jax.ShapeDtypeStruct((2048, 512)...]
    all_to_all x1, waiting for transfers between devices: 26.1 us -> 0.01 us  [copy_for_each(): lax.all_to_all(jnp.broadcast_to(value[None], (count, *value.shape)), axis...]
    all_to_all x2, blocking collectives: 78.9 us -> 65.3 us  [sum_at_owner(): lax.all_to_all(cut_along(value, dim, count), axis, 0, 0, tiled=True)]
    unnamed x22 -> x21, local copies, waits for them, and re-layouts: 6.96 us -> 5.04 us
  transfers between devices with their start and end apart: 2 -> 1, of which waited for: 2 -> 0; matrix products, arithmetic and copies ran while one was open for 2% -> 0% of each run, Pallas kernels for 0% -> 34%
where the time goes in v1:
time: 203 us
  blocking collectives  94.9 us (47%)
  Pallas kernels  69.4 us (34%)
  matrix products  12.8 us (6%)
  starting transfers between devices  10.5 us (5%)
  other arithmetic  7.2 us (4%)
  local copies, waits for them, and re-layouts  7.16 us (4%)
    pallas_call x1, Pallas kernels, gather_units(): pl.pallas_call(gather_kernel, out_shape=[jax.ShapeDtypeStruct((2048, 512)...  69.4 us
    all_to_all x2, blocking collectives, sum_at_owner(): lax.all_to_all(cut_along(value, dim, count), axis, 0, 0, tiled=True)  65.3 us
    all_to_all x1, blocking collectives, copy_for_each(): lax.all_to_all(jnp.broadcast_to(value[None], (count, *value.shape)), axis...  29.7 us
    all_to_all x1, starting transfers between devices, copy_for_each(): lax.all_to_all(jnp.broadcast_to(value[None], (count, *value.shape)), axis...  10.5 us
    dot_general x1, matrix products, shards(): chan_terms = jnp.dot(hidden, down_all, preferred_element_type=jnp.float32)  5.21 us
    unnamed x21, local copies, waits for them, and re-layouts  5.04 us
  transfers between devices with their start and end apart: 1, of which 0 were waited for; matrix products, arithmetic and copies ran while one was open for 0% of the time, Pallas kernels for 34%

profile of v1, /device:TPU:1, one launch (start us, length us, event | category | flops | bytes accessed | tf_op | source)
XLA Modules:
  0.0 202.6 jit_solution(9260244959543837694)
XLA Ops:
  0.0 1.1 copy.23
  1.1 1.5 broadcast_in_dim.15
  2.6 10.5 %all-to-all-start = ((bf16[8,512,256]{1,2,0:T(8,128)(2,1)}), bf16[8,512,256]{1,2,0:T(8,128)(2,1)S(1)}, u32[]{:S(2)}, u32[]{:S(2)}) async-start(bf16[8,512,256]{1,2,0:T(8,128)(2,1)} %broadcast_in_dim.15), calls=%async_computation | async-start | bytes 4194304 | tf_op jit(solution)/shard_map/all_to_all | solution.py:173
  13.3 0.6 pad_maximum_fusion.1.refs_0_
  13.9 69.4 %gather_units.1 = (bf16[2048,512]{1,0:T(8,128)(2,1)}, bf16[2048,512]{1,0:T(8,128)(2,1)}, bf16[2048,512]{1,0:T(8,128)(2,1)}, bf16[2048,512]{1,0:T(8,128)(2,1)}, bf16[2048,512]{1,0:T(8,128)(2,1)}) custom-call(bf16[64,512]{1,0:T(8,128)(2,1)} %pad_maximum_fusion.1.refs_0_, bf16[64,512]{1,0:T(8,128)(2,1)} %refs_1_.1, bf16[64,512]{1,0:T(8,128)(2,1)} %bitcast.159, ...), custom_call_target="tpu_custom_call" | custom-call | tf_op jit(solution)/shard_map/gather_units/pallas_call | solution.py:148
  83.4 0.5 multiply_reduce_fusion.1
  83.9 0.5 fusion.57
  84.5 1.0 copy-done.9
  85.5 0.8 convolution_bitcast_fusion.1
  86.3 0.8 convolution_bitcast_fusion.2
  87.1 0.8 copy-done.2
  87.9 1.3 convolution_convert_fusion.2
  89.2 1.2 fusion.77
  90.5 3.8 %while.15 = (s32[]{:T(128)}, f32[1,256,512]{2,1,0:T(8,128)S(1)}, f32[4,1,128,512]{3,2,1,0:T(8,128)S(1)}, f32[1]{0:T(128)}, bf16[4,1,128,256]{3,2,1,0:T(8,128)(2,...) while((s32[]{:T(128)}, f32[1,256,512]{2,1,0:T(8,128)S(1)}, ...), condition=%wide.region_2.3_spmd.clone.clone.clone, body=%wide.region_1.2_spmd.clone.clone.clone.sunk | while | flops 93176320 | bytes 2890370 | solution.py:241
  90.5 0.3 fusion.108
  91.1 0.3 fusion.107
  91.5 0.3 fusion.108
  92.1 0.3 fusion.107
  92.4 0.3 fusion.108
  93.0 0.3 fusion.107
  93.4 0.3 fusion.108
  94.0 0.3 fusion.107
  94.6 1.2 copy-done.8
  95.9 1.3 convolution_convert_fusion.1
  97.3 35.6 %all_to_all.20 = bf16[8,512,256]{2,1,0:T(8,128)(2,1)S(1)} all-to-all(bf16[8,512,256]{2,1,0:T(8,128)(2,1)S(1)} %bitcast.150), channel_id=1, replica_groups=mesh['rep'=2,'fs'=32,'tp'=8] {'tp'}, dimensions={0} | all-to-all | bytes 4194304 | tf_op jit(solution)/shard_map/all_to_all | solution.py:190
  133.2 0.6 copy-done.3
  134.3 29.7 %all_to_all.21 = bf16[8,512,256]{1,2,0:T(8,128)(2,1)S(1)} all-to-all(bf16[8,512,256]{1,2,0:T(8,128)(2,1)S(1)} %broadcast_in_dim.16), channel_id=1, replica_groups=mesh['rep'=2,'fs'=32,'tp'=8] {'tp'}, dimensions={0} | all-to-all | bytes 4194304 | tf_op jit(solution)/shard_map/all_to_all | solution.py:173
  163.9 0.5 multiply_reduce_fusion
  164.6 1.9 fusion.55
  166.5 5.2 %convolution_convert_fusion = bf16[512,2048]{1,0:T(8,128)(2,1)S(1)} fusion(bf16[2048,512]{1,0:T(8,128)(2,1)} %get-tuple-element.67, bf16[512,2048]{0,1:T(8,128)(2,1)} %fusion.55, bf16[2048,512]{1,0:T(8,128)(2,1)} %get-tuple-element.66), kind=kOutput, calls=%fused_computation.61 | convolution fusion | flops 2149318656 | bytes 8388608 | tf_op jit(solution)/shard_map/dot_general | solution.py:275
  171.9 29.7 %all_to_all.22 = bf16[8,512,256]{2,1,0:T(8,128)(2,1)S(1)} all-to-all(bf16[8,512,256]{2,1,0:T(8,128)(2,1)S(1)} %bitcast.151), channel_id=1, replica_groups=mesh['rep'=2,'fs'=32,'tp'=8] {'tp'}, dimensions={0} | all-to-all | bytes 4194304 | tf_op jit(solution)/shard_map/all_to_all | solution.py:190
  201.8 0.8 add_convert_fusion
  (44 shorter events, 2.8 us)
Async XLA Ops:
  0.0 83.4 %copy-start = (f32[8,512]{1,0:T(8,128)S(1)}, f32[8,512]{1,0:T(8,128)}, u32[]{:S(2)}) copy-start(f32[8,512]{1,0:T(8,128)} %param.17) | copy-start | bytes 49156
  2.6 10.6 %copy-start.4 = (bf16[64,256]{1,0:T(8,128)(2,1)S(1)}, bf16[64,256]{1,0:T(8,128)(2,1)}, u32[]{:S(2)}) copy-start(bf16[64,256]{1,0:T(8,128)(2,1)} %param.15) | copy-start | bytes 98308
  2.6 10.6 %copy-start.5 = (bf16[64,256]{1,0:T(8,128)(2,1)S(1)}, bf16[64,256]{1,0:T(8,128)(2,1)}, u32[]{:S(2)}) copy-start(bf16[64,256]{1,0:T(8,128)(2,1)} %param.14) | copy-start | bytes 98308
  2.6 80.8 %all-to-all-start = ((bf16[8,512,256]{1,2,0:T(8,128)(2,1)}), bf16[8,512,256]{1,2,0:T(8,128)(2,1)S(1)}, u32[]{:S(2)}, u32[]{:S(2)}) async-start(bf16[8,512,256]{1,2,0:T(8,128)(2,1)} %broadcast_in_dim.15), calls=%async_computation | async-start | bytes 4194304 | tf_op jit(solution)/shard_map/all_to_all | solution.py:173
  13.1 70.8 %copy-start.6 = (f32[2048]{0:T(1024)S(1)}, f32[2048]{0:T(1024)}, u32[]{:S(2)}) copy-start(f32[2048]{0:T(1024)} %param.13) | copy-start | bytes 24580
  83.9 1.6 copy-start.9
  86.3 1.6 copy-start.2
  89.1 1.3 copy-start.1
  94.3 1.6 copy-start.8
  132.9 1.0 copy-start.3
  163.9 0.7 copy-start.7

commit v2 on v1

v2 whole, which is shorter than its diff:
```python
import heapq

import jax
import jax.numpy as jnp
import numpy as np
from jax import lax
from jax.experimental import pallas as pl
from jax.experimental.pallas import tpu as pltpu
from jax.sharding import PartitionSpec as P

ROWS = 512
D = 2048
DK = 256
DV = 512
EPS = 1e-06
HEAD_EPS = 0.05
THETA = 10000.0
NX, NY, NZ = 4, 8, 4
ROUTES = "ABABA"
GROUPS = (0, 0, 1, 2, 2)
STARTS = (0.0, 0.0, 3.0, 3.0, 3.0)
MESH = pl.DeviceIdType.MESH
BF, F32 = jnp.bfloat16, jnp.float32


def neighbours(route, a, b, unit):
    out = []
    two = lambda k: 1 if k % 2 == 0 else -1
    if route == "A":
        fw = 4 if unit % 4 < 2 else 3
        bw = 7 - fw
        if b == 0:
            if 0 <= a < fw: out.append(("y", 1))
            if 0 >= a > -bw: out.append(("y", -1))
            out += [("z", 1), ("z", -1)]
        elif abs(b) == 1 and two(a) == b:
            out.append(("z", b))
    else:
        fw = 4 if b % 2 == 0 else 3
        bw = 7 - fw
        if a == 0:
            if b == 0: out += [("z", 1), ("z", -1)]
            elif abs(b) == 1 and two(unit // 2) == b: out.append(("z", b))
        if 0 <= a < fw: out.append(("y", 1))
        if 0 >= a > -bw: out.append(("y", -1))
    return out

def simulate(routes, group, service=1.45, latency=1.8, lead=3.2, start=None):
    start = start or [0.0] * len(routes)
    def down(u, a, b):
        n = neighbours(routes[u], a, b, u)
        return max([0] + [1 + down(u, a + (s if ax == "y" else 0), b + (s if ax == "z" else 0)) for ax, s in n])
    free = {(ax, s): 0.0 for ax in "yz" for s in (1, -1)}
    pending = {k: [] for k in free}
    events = []
    actions = []
    seq = 0
    arrivals = [(start[u], 0, u, 0, 0) for u in range(len(routes))]
    heapq.heapify(arrivals)
    index = {}
    counts = [0] * len(routes)
    now = 0.0
    arrived = {}
    while arrivals or any(pending.values()):
        t_link = min([max(free[k], min(p[2] for p in pending[k])) for k in free if pending[k]], default=float("inf"))
        t_arr = arrivals[0][0] if arrivals else float("inf")
        if t_arr <= t_link:
            t, hop, u, a, b = heapq.heappop(arrivals)
            arrived[(u, a, b)] = t
            if (a, b) != (0, 0):
                index[(u, a, b)] = counts[u]; counts[u] += 1
                actions.append((t, 0, ("wait", u, a, b)))
            for ax, s in neighbours(routes[u], a, b, u):
                na, nb = a + (s if ax == "y" else 0), b + (s if ax == "z" else 0)
                pending[(ax, s)].append((group[u], -(1 + down(u, na, nb)), t, u, a, b, na, nb))
        else:
            k = min((k for k in free if pending[k]), key=lambda k: max(free[k], min(p[2] for p in pending[k])))
            t0 = t_link
            ready = [p for p in pending[k] if p[2] <= t0 + 1e-9]
            p = min(ready)
            pending[k].remove(p)
            free[k] = t0 + service
            g, d, t, u, a, b, na, nb = p
            actions.append((max(t, t0 - lead), 1, ("send", u, a, b, na, nb, k)))
            heapq.heappush(arrivals, (t0 + service + latency, 1, u, na, nb))
    actions.sort(key=lambda x: (x[0], x[1]))
    return actions, index, counts, arrived


def turned_dot(left, right):
    return lax.dot_general(left, right, (((1,), (1,)), ((), ())), preferred_element_type=F32)


def layer_kernel(
    tokens, mix_gain, query_w, key_w, value_w, head_gain, out_w, chan_gain, up_w, down_w, cosine, sine,
    result,
    w_both, w_value, w_out, w_up, w_down,
    blocks, normed, middle, turn_in, mix_row, chan_row, head_rows, cos_tab, sin_tab, decay,
    raw, query, keys, values, head_out, hidden,
    give1, take1, own1, move1, plain1, left1, right1, pass1,
    give2, take2, own2, move2, left2, right2, pass2,
    local_sem, send_sem, recv_sem,
):
    rep, fs, tp = lax.axis_index("rep"), lax.axis_index("fs"), lax.axis_index("tp")
    z, y = fs // NY, fs % NY
    x, core = tp // 2, tp % 2
    units = (w_both, w_value, w_out, w_up, w_down)
    target = {
        ("y", 1): {"fs": z * NY + (y + 1) % NY},
        ("y", -1): {"fs": z * NY + (y + NY - 1) % NY},
        ("z", 1): {"rep": (rep + (z + 1) // NZ) % 2, "fs": ((z + 1) % NZ) * NY + y},
        ("z", -1): {"rep": (rep + (NZ - z) // NZ) % 2, "fs": ((z + NZ - 1) % NZ) * NY + y},
        "right": {"tp": ((x + 1) % NX) * 2 + core},
        "left": {"tp": ((x + NX - 1) % NX) * 2 + core},
        "partner": {"tp": x * 2 + (1 - core)},
    }
    barrier = pltpu.get_barrier_semaphore()
    for k in target:
        pl.semaphore_signal(barrier, inc=1, device_id=target[k], device_id_type=MESH)

    def slot(a, b):
        at = ((z - b + NZ) % NZ) * NY + (y - a + NY) % NY
        return pl.ds(pl.multiple_of(at * 64, 64), 64)

    mine = slot(0, 0)
    local = []

    def bring(source, dest):
        copy = pltpu.make_async_copy(source, dest, local_sem.at[len(local)])
        copy.start()
        local.append(copy)

    bring(tokens, blocks.at[tp])
    bring(query_w, w_both.at[mine, 0:DK])
    bring(key_w, w_both.at[mine, DK : 2 * DK])
    bring(value_w, w_value.at[mine])
    bring(out_w, turn_in.at[0])
    bring(down_w, turn_in.at[1])
    bring(up_w, w_up.at[mine])
    bring(mix_gain, mix_row)
    bring(chan_gain, chan_row)
    bring(head_gain, head_rows)
    bring(cosine, cos_tab)
    bring(sine, sin_tab)
    for copy in local[:4]:
        copy.wait()
    pl.semaphore_wait(barrier, len(target))

    sends, names = [], {}

    def number(name):
        return names.setdefault(name, len(names))

    def send(source, dest, to, name):
        copy = pltpu.make_async_remote_copy(
            src_ref=source,
            dst_ref=dest,
            send_sem=send_sem.at[len(sends)],
            recv_sem=recv_sem.at[number(name)],
            device_id=target[to],
            device_id_type=MESH,
        )
        copy.start()
        sends.append(copy)

    def arrive(dest, name):
        pltpu.make_async_copy(dest, dest, recv_sem.at[number(name)]).wait()

    actions = simulate(ROUTES, GROUPS, start=STARTS)[0]
    position = [0]
    turned = []

    def turn():
        for copy in local[4:]:
            copy.wait()
        w_out[mine, :] = turn_in[0].T
        w_down[mine, :] = turn_in[1].T

    def step_weights():
        _, _, action = actions[position[0]]
        position[0] += 1
        if action[0] == "wait":
            _, u, a, b = action
            arrive(units[u].at[slot(a, b)], ("w", u, a, b))
        else:
            _, u, a, b, na, nb, k = action
            send(units[u].at[slot(a, b)], units[u].at[slot(a, b)], k, ("w", u, na, nb))

    def at(time):
        while position[0] < len(actions) and actions[position[0]][0] <= time:
            step_weights()

    def need(u, planes=(0, 1, -1, 2, -2)):
        last = max(i for i, c in enumerate(actions) if c[2][0] == "wait" and c[2][1] == u and c[2][3] in planes)
        while position[0] <= last:
            step_weights()

    def block_of(o, c):
        return ((x + o + NX) % NX) * 2 + c

    def gather(view, tag, times, arrived=None):
        def to(o, h, k, name):
            send(view(o, core, h), view(o, core, h), k, (tag, *name))

        to(0, 0, "right", (-1, 0))
        to(0, 1, "left", (1, 1))
        to(0, 1, "right", (-1, 1))
        to(0, 0, "left", (1, 0))
        to(0, 0, "partner", ("p", 0, 0))
        to(0, 1, "partner", ("p", 0, 1))
        order = [(-1, 0), (1, 1), (-1, 1), (1, 0), (-2, 0), (2, 1)]
        for (o, h), time in zip(order, times):
            at(time)
            arrive(view(o, core, h), (tag, o, h))
            if (o, h) == (-1, 0):
                to(o, h, "right", (-2, 0))
            if (o, h) == (1, 1):
                to(o, h, "left", (2, 1))
            to(o, h, "partner", ("p", o, h))
            if arrived and (o, h) in ((-1, 1), (1, 0), (2, 1)):
                arrived(o, core)
        for o, h in [(0, 0), (0, 1)] + order:
            arrive(view(o, 1 - core, h), (tag, "p", o, h))
            if arrived and (o, h) in ((0, 1), (-1, 1), (1, 0), (2, 1)):
                arrived(o, 1 - core)

    def token_view(o, c, h):
        return blocks.at[block_of(o, c), pl.ds(h * 256, 256)]

    at(0.0)
    rate = jnp.float32(0.0)
    for h in range(8):
        rate = jnp.where(tp == h, jnp.float32(np.log1p(-(2.0 ** (-5 - h)))), rate)
    gather_times = (5.0, 5.2, 7.8, 8.0, 10.6, 10.8)

    started = [False]

    def begin():
        turn()
        offset = (
            lax.broadcasted_iota(jnp.int32, (128, 128), 0) - lax.broadcasted_iota(jnp.int32, (128, 128), 1)
        ).astype(F32)
        for n in range(4):
            value = jnp.exp(rate * jnp.maximum(offset + 128.0 * n, 0.0))
            decay[n] = jnp.where(offset + 128.0 * n >= 0, value, 0.0)

    begin()
    gather(token_view, "t", gather_times)

    at(12.0)

    @pl.loop(0, ROWS // 64)
    def _(i):
        rows = pl.ds(pl.multiple_of(i * 64, 64), 64)
        total = jnp.zeros((64, 256), F32)
        for b in range(8):
            part = blocks[b, rows, :].astype(F32)
            total = total + part * part
        scale = lax.rsqrt(jnp.sum(total, axis=-1, keepdims=True) * (1.0 / D) + EPS)
        for b in range(8):
            columns = slice(b * 256, (b + 1) * 256)
            normed[rows, columns] = (blocks[b, rows, :].astype(F32) * scale * mix_row[:, columns]).astype(BF)

    def project(weights, tile, store):
        @pl.loop(0, 512 // tile)
        def _(i):
            columns = pl.ds(pl.multiple_of(i * tile, tile), tile)
            store(columns, jnp.dot(normed[...], weights[:, columns], preferred_element_type=F32))

    def keep_raw(columns, value):
        raw[:, columns] = value

    def keep_values(columns, value):
        values[:, columns] = value.astype(BF)

    def keep_hidden(columns, value):
        value = jnp.maximum(value, 0.0)
        hidden[:, columns] = (value * value).astype(BF)

    need(0)
    project(w_both, 256, keep_raw)
    need(1)
    at(31.0)
    project(w_value, 256, keep_values)

    @pl.loop(0, ROWS // 64)
    def _(i):
        rows = pl.ds(pl.multiple_of(i * 64, 64), 64)
        c, s = cos_tab[rows, :], sin_tab[rows, :]
        for start, dest, factor in ((0, query, 1.0), (DK, keys, DK**-0.5)):
            first, second = raw[rows, start : start + 128], raw[rows, start + 128 : start + 256]
            dest[rows, 0:128] = ((first * c - second * s) * factor).astype(BF)
            dest[rows, 128:256] = ((second * c + first * s) * factor).astype(BF)

    at(33.0)
    gain = head_rows[pl.ds(tp, 1), :]
    for i in range(4):
        rows = slice(i * 128, (i + 1) * 128)
        total = jnp.zeros((128, DV), F32)
        for j in range(i + 1):
            there = slice(j * 128, (j + 1) * 128)
            score = turned_dot(query[rows, :], keys[there, :]) * decay[i - j]
            total = total + jnp.dot(score.astype(BF), values[there, :], preferred_element_type=F32)
        scale = lax.rsqrt(jnp.mean(total * total, axis=-1, keepdims=True) + HEAD_EPS)
        part = (total * scale * gain).astype(BF)
        head_out[i, 0] = part[0:64]
        head_out[i, 1] = part[64:128]
        at(33.0 + 0.4 * (i + 1))

    planes = (0, 1, -1, 2)
    reached = {0: (0,), 1: (1,), -1: (-1,), 2: (2, -2)}

    def plane(b):
        return (z - b + NZ) % NZ

    def offset_rows(o, h):
        return pl.ds(pl.multiple_of(((x + o + NX) % NX) * 64 + h * 32, 32), 32)

    def exchange(n, b):
        weights = w_out[pl.ds(pl.multiple_of(plane(b) * 512, 512), 512), :]
        give1[n] = turned_dot(head_out[:, 1 - core].reshape(256, 512), weights).astype(BF)
        own1[n] = turned_dot(head_out[:, core].reshape(256, 512), weights)
        send(give1.at[n], take1.at[n], "partner", ("m", n))

    def part(n, o, h):
        rows = offset_rows(o, h)
        return own1[n, rows, :] + take1[n, rows, :].astype(F32)

    half = (slice(0, 32), slice(32, 64))

    def spread(n):
        arrive(take1.at[n], ("m", n))
        move1[n, 0] = part(n, 2, 0).astype(BF)
        move1[n, 1] = part(n, 2, 1).astype(BF)
        plain1[n, 0] = part(n, 1, 1).astype(BF)
        plain1[n, 1] = part(n, -1, 0).astype(BF)
        send(move1.at[n, 0], pass1.at[n, 0], "right", ("m2", n, 0))
        send(move1.at[n, 1], pass1.at[n, 1], "left", ("m2", n, 1))
        send(plain1.at[n, 0], left1.at[n, half[1]], "right", ("m1", n, 0))
        send(plain1.at[n, 1], right1.at[n, half[0]], "left", ("m1", n, 1))

    def merge(n):
        arrive(pass1.at[n, 0], ("m2", n, 0))
        move1[n, 2] = (part(n, 1, 0) + pass1[n, 0].astype(F32)).astype(BF)
        arrive(pass1.at[n, 1], ("m2", n, 1))
        move1[n, 3] = (part(n, -1, 1) + pass1[n, 1].astype(F32)).astype(BF)
        send(move1.at[n, 2], left1.at[n, half[0]], "right", ("m3", n, 0))
        send(move1.at[n, 3], right1.at[n, half[1]], "left", ("m3", n, 1))

    my_rows = pl.ds(pl.multiple_of(tp * 64, 64), 64)

    def settle(n, b):
        arrive(left1.at[n, half[1]], ("m1", n, 0))
        arrive(right1.at[n, half[0]], ("m1", n, 1))
        arrive(left1.at[n, half[0]], ("m3", n, 0))
        arrive(right1.at[n, half[1]], ("m3", n, 1))
        rows = pl.ds(pl.multiple_of(x * 64, 64), 64)
        total = own1[n, rows, :] + take1[n, rows, :].astype(F32)
        total = total + left1[n].astype(F32) + right1[n].astype(F32)
        for j in range(2):
            here = total[:, j * 256 : (j + 1) * 256] + blocks[2 * plane(b) + j, my_rows, :].astype(F32)
            columns = pl.ds(pl.multiple_of(plane(b) * 512 + j * 256, 256), 256)
            middle[my_rows, columns] = here.astype(BF)

    for n, b in enumerate(planes):
        need(2, reached[b])
        exchange(n, b)
        if n >= 1:
            spread(n - 1)
        if n >= 2:
            merge(n - 2)
    base = 46.0
    at(base + 1.0)
    spread(3)
    at(base + 2.0)
    merge(2)
    at(base + 4.0)
    merge(3)
    for n, b in enumerate(planes):
        at(base + 4.0 + n)
        settle(n, b)

    def middle_view(o, c, h):
        return middle.at[pl.ds(pl.multiple_of(block_of(o, c) * 64 + h * 32, 32), 32)]

    def norm_block(o, c):
        rows = pl.ds(pl.multiple_of(block_of(o, c) * 64, 64), 64)
        total = jnp.zeros((64, 256), F32)
        for b in range(8):
            chunk = middle[rows, b * 256 : (b + 1) * 256].astype(F32)
            total = total + chunk * chunk
        scale = lax.rsqrt(jnp.sum(total, axis=-1, keepdims=True) * (1.0 / D) + EPS)
        for b in range(8):
            columns = slice(b * 256, (b + 1) * 256)
            normed[rows, columns] = (middle[rows, columns].astype(F32) * scale * chan_row[:, columns]).astype(BF)

    base = 52.0
    at(base)
    gather(middle_view, "c", [base + t for t in gather_times], norm_block)
    norm_block(0, core)

    need(3)
    at(64.0)
    project(w_up, 256, keep_hidden)

    need(4)
    around = (2, 1, -1, 0)

    def terms(o, c):
        return turned_dot(hidden[...], w_down[pl.ds(pl.multiple_of(block_of(o, c) * 256, 256), 256), :])

    halves = (slice(0, 256), slice(256, 512))
    for n, o in enumerate(around):
        give2[n] = terms(o, 1 - core).astype(BF)
        send(give2.at[n], take2.at[n], "partner", ("d", n))

    def summed(n):
        arrive(take2.at[n], ("d", n))
        own2[...] = terms(around[n], core) + take2[n].astype(F32)

    summed(0)
    move2[0] = own2[halves[0], :].astype(BF)
    move2[1] = own2[halves[1], :].astype(BF)
    send(move2.at[0], pass2.at[0], "right", ("d2", 0))
    send(move2.at[1], pass2.at[1], "left", ("d2", 1))
    summed(1)
    move2[2] = own2[halves[1], :].astype(BF)
    move2[4] = own2[halves[0], :].astype(BF)
    send(move2.at[2], left2.at[halves[1]], "right", ("d1", 0))
    summed(2)
    move2[3] = own2[halves[0], :].astype(BF)
    move2[5] = own2[halves[1], :].astype(BF)
    send(move2.at[3], right2.at[halves[0]], "left", ("d1", 1))
    arrive(pass2.at[0], ("d2", 0))
    move2[4] = (move2[4].astype(F32) + pass2[0].astype(F32)).astype(BF)
    send(move2.at[4], left2.at[halves[0]], "right", ("d3", 0))
    arrive(pass2.at[1], ("d2", 1))
    move2[5] = (move2[5].astype(F32) + pass2[1].astype(F32)).astype(BF)
    send(move2.at[5], right2.at[halves[1]], "left", ("d3", 1))
    summed(3)
    own2[...] += middle[:, pl.ds(pl.multiple_of(tp * 256, 256), 256)].astype(F32)
    arrive(left2.at[halves[1]], ("d1", 0))
    arrive(right2.at[halves[0]], ("d1", 1))
    arrive(left2.at[halves[0]], ("d3", 0))
    arrive(right2.at[halves[1]], ("d3", 1))
    result[...] = (own2[...] + left2[...].astype(F32) + right2[...].astype(F32)).astype(BF)
    at(1000.0)
    for copy in sends:
        copy.wait_send()


def rotary_tables():
    half = DK // 2
    angle = np.arange(ROWS)[:, None] * THETA ** (-np.arange(half) / half)
    return np.cos(angle).astype(np.float32), np.sin(angle).astype(np.float32)


def shards(tokens, mix_gain, query_w, key_w, value_w, head_gain, out_w, chan_gain, up_w, down_w):
    cosine, sine = rotary_tables()
    any_place = pl.BlockSpec(memory_space=pl.ANY)
    vmem = pltpu.VMEM
    scratch = [
        *[vmem((D, 512), BF)] * 5,
        vmem((8, ROWS, 256), BF),
        vmem((ROWS, D), BF),
        vmem((ROWS, D), BF),
        vmem((2, 512, 64), BF),
        vmem((1, D), F32),
        vmem((1, D), F32),
        vmem((8, DV), F32),
        vmem((ROWS, DK // 2), F32),
        vmem((ROWS, DK // 2), F32),
        vmem((4, 128, 128), F32),
        vmem((ROWS, 512), F32),
        vmem((ROWS, DK), BF),
        vmem((ROWS, DK), BF),
        vmem((ROWS, DV), BF),
        vmem((4, 2, 64, DV), BF),
        vmem((ROWS, 512), BF),
        vmem((4, 256, 512), BF),
        vmem((4, 256, 512), BF),
        vmem((4, 256, 512), F32),
        vmem((4, 4, 32, 512), BF),
        vmem((4, 2, 32, 512), BF),
        vmem((4, 64, 512), BF),
        vmem((4, 64, 512), BF),
        vmem((4, 2, 32, 512), BF),
        vmem((4, ROWS, 256), BF),
        vmem((4, ROWS, 256), BF),
        vmem((ROWS, 256), F32),
        vmem((6, 256, 256), BF),
        vmem((ROWS, 256), BF),
        vmem((ROWS, 256), BF),
        vmem((2, 256, 256), BF),
        pltpu.SemaphoreType.DMA((12,)),
        pltpu.SemaphoreType.DMA((260,)),
        pltpu.SemaphoreType.DMA((260,)),
    ]
    return pl.pallas_call(
        layer_kernel,
        out_shape=jax.ShapeDtypeStruct((ROWS, 256), BF),
        in_specs=[any_place] * 12,
        out_specs=pl.BlockSpec(memory_space=pltpu.VMEM),
        scratch_shapes=scratch,
        compiler_params=pltpu.CompilerParams(
            collective_id=0, has_side_effects=True, vmem_limit_bytes=60 << 20
        ),
        name="layer",
    )(
        tokens, mix_gain.reshape(1, D), query_w, key_w, value_w, head_gain, out_w,
        chan_gain.reshape(1, D), up_w, down_w, jnp.asarray(cosine), jnp.asarray(sine),
    )


def solution(mesh):
    placed = (
        P(("rep", "fs"), "tp"),
        P(),
        P("fs", "tp"),
        P("fs", "tp"),
        P("fs", "tp"),
        P(),
        P("tp", "fs"),
        P(),
        P("fs", "tp"),
        P("tp", "fs"),
    )
    return jax.shard_map(
        shards, mesh=mesh, in_specs=placed, out_specs=P(("rep", "fs"), "tp"), check_vma=False
    )
```

time: 203 us -> 113 us (0.56)
  blocking collectives: 94.9 us -> 0 us
  Pallas kernels: 69.4 us -> 109 us
  matrix products: 12.8 us -> 0 us
  starting transfers between devices: 10.5 us -> 0 us
  other arithmetic: 7.2 us -> 0 us
  local copies, waits for them, and re-layouts: 7.16 us -> 4.06 us
    all_to_all x3 -> x0, blocking collectives: 94.9 us -> none  [the longest x2 65.3 us: sum_at_owner(): lax.all_to_all(cut_along(value, dim, count), axis, 0, 0, tiled=True)]
    pallas_call x1, Pallas kernels: 69.4 us -> 109 us  [shards(): pl.pallas_call(layer_kernel, out_shape=jax.ShapeDtypeStruct((ROWS, 256),...]
    dot_general x17 -> x0, matrix products: 12.8 us -> none  [the longest x1 5.21 us: shards(): chan_terms = jnp.dot(hidden, down_all, preferred_element_type=jnp.float32)]
    all_to_all x1 -> x0, starting transfers between devices: 10.5 us -> none  [copy_for_each(): lax.all_to_all(jnp.broadcast_to(value[None], (count, *value.shape)), axis...]
    convert_element_type x7 -> x0, other arithmetic: 3.43 us -> none  [the longest x2 2.41 us: norm_rows(): return (values * scale * gain).astype(jnp.bfloat16)]
    unnamed x21 -> x5, local copies, waits for them, and re-layouts: 5.04 us -> 4.06 us
  transfers between devices with their start and end apart: 1 -> 0, of which waited for: 0 -> 0; matrix products, arithmetic and copies ran while one was open for 0% -> 0% of each run, Pallas kernels for 34% -> 0%
where the time goes in v2:
time: 113 us
  Pallas kernels  109 us (96%)
  local copies, waits for them, and re-layouts  4.06 us (4%)
    pallas_call x1, Pallas kernels, shards(): pl.pallas_call(layer_kernel, out_shape=jax.ShapeDtypeStruct((ROWS, 256),...  109 us
    unnamed x5, local copies, waits for them, and re-layouts  4.06 us

profile of v2, /device:TPU:1, one launch (start us, length us, event | category | flops | bytes accessed | tf_op | source)
XLA Modules:
  0.0 113.2 jit_solution(9497750431392652569)
XLA Ops:
  0.0 0.0 copy-start
  0.0 1.6 %copy.13.out_w = bf16[512,64]{1,0:T(8,128)(2,1)} copy(bf16[512,64]{0,1:T(8,128)(2,1)} %param.18) | data formatting | bytes 131072 | tf_op args[6]
  1.6 0.0 copy-done
  1.6 0.8 copy.14.down_w
  2.4 109.1 %layer.1 = bf16[512,256]{1,0:T(8,128)(2,1)} custom-call(bf16[512,256]{1,0:T(8,128)(2,1)} %tokens.1, f32[1,2048]{1,0:T(1,128)} %bitcast.2, bf16[64,256]{1,0:T(8,128)(2,1)} %query_w.1, bf16[64,256]{1,0:T(8,128)(2,1)} %key_w.1, bf16[64,512]{1,0:T(8,128)(2,1)} %value_w.1, f32[8,512]{1,0:T(8,128)} %head_gain.1, bf16[512,64]{1,0:T(8,128)(2,1)} %copy.13.out_w, ...), custom_call_target="tpu_custom_call" | custom-call | tf_op jit(solution)/shard_map/layer/pallas_call | solution.py:499
  111.5 1.7 %copy.16 = bf16[512,256]{1,0:T(8,128)(2,1)} copy(bf16[512,256]{1,0:T(8,128)(2,1)} %layer.1) | data formatting | bytes 524288
Async XLA Ops:
  0.0 1.6 %copy-start = (bf16[512,64]{0,1:T(8,128)(2,1)S(1)}, bf16[512,64]{0,1:T(8,128)(2,1)}, u32[]{:S(2)}) copy-start(bf16[512,64]{0,1:T(8,128)(2,1)} %param.21) | copy-start | bytes 196612

commit v3 on v0

v3 whole, which is shorter than its diff:
```python
import heapq
from collections import defaultdict

import jax
import jax.numpy as jnp
import numpy as np
from jax import lax
from jax.experimental import pallas as pl
from jax.experimental.pallas import tpu as pltpu
from jax.sharding import PartitionSpec as P

ROWS = 512
D = 2048
DK = 256
DV = 512
EPS = 1e-06
HEAD_EPS = 0.05
THETA = 10000.0
NX, NY, NZ = 4, 8, 4
MESH = pl.DeviceIdType.MESH
BF, F32 = jnp.bfloat16, jnp.float32

PARTS = (
    (0, 0, 64, "A", 0, 0.0),
    (1, 0, 64, "B", 1, 0.0),
    (2, 0, 64, "A", 1, 1.0),
    (3, 0, 32, "A", 2, 2.5),
    (3, 32, 32, "B", 2, 2.5),
    (4, 0, 32, "A", 2, 2.5),
    (4, 32, 32, "B", 2, 2.5),
)
SENDS, LANDS = 13, 220
LEAD = {"y": 3.2, "z": 3.2, "x": 2.0}
XRANK = {(t, i): (i + 1.5 * k, k) for k, t in enumerate("mcd") for i in range(4)}
RATE = {"ring": 45.2e3, "partner": 600e3}
DELAY = {"early": 2.3, "late": 3.0, "x": 2.2, "partner": 1.1}


def onward(p, a, b):
    out = []
    two = lambda k: 1 if k % 2 == 0 else -1
    if PARTS[p][3] == "A":
        fw = 4 if p % 4 < 2 else 3
        if b == 0:
            if 0 <= a < fw:
                out.append(("y", 1))
            if 0 >= a > fw - 7:
                out.append(("y", -1))
            out += [("z", 1), ("z", -1)]
        elif abs(b) == 1 and two(a) == b:
            out.append(("z", b))
    else:
        fw = 4 if b % 2 == 0 else 3
        if a == 0:
            if b == 0:
                out += [("z", 1), ("z", -1)]
            elif abs(b) == 1 and two(p // 2) == b:
                out.append(("z", b))
        if 0 <= a < fw:
            out.append(("y", 1))
        if 0 >= a > fw - 7:
            out.append(("y", -1))
    return [(k, a + k[1] * (k[0] == "y"), b + k[1] * (k[0] == "z")) for k in out]


def below(p, a, b):
    return max([0] + [1 + below(p, na, nb) for _, na, nb in onward(p, a, b)])


def schedule(tasks, messages):
    left, users, leaving = {}, defaultdict(list), defaultdict(list)
    for name, (needs, _, _, start) in tasks.items():
        left[name] = len(needs) + 1
        for need in needs:
            users[need].append(name)
    for name, (task, *_) in messages.items():
        leaving[task].append(name)
    events, ready, items = [], [], []
    count = 0
    link_free = defaultdict(float)
    queue = defaultdict(list)
    core_free = 0.0
    for name, (_, _, _, start) in tasks.items():
        heapq.heappush(events, (start, count, "part", name))
        count += 1
    now = 0.0

    def serve(link, time):
        nonlocal count
        while queue[link] and link_free[link] <= time + 1e-9:
            message = heapq.heappop(queue[link])[-1]
            kind = "partner" if link == "partner" else "ring"
            begin = max(time, link_free[link])
            link_free[link] = begin + messages[message][2] / RATE[kind]
            if messages[message][3] is not None:
                items.append((max(available[message], begin - LEAD[link[0]]), 1, len(items), "send", message))
            rank = messages[message][3]
            delay = DELAY["partner" if link == "partner" else "x" if link[0] == "x" else "early" if rank[0] < 2 else "late"]
            heapq.heappush(events, (link_free[link] + delay, count, "arrive", message))
            heapq.heappush(events, (link_free[link], count + 1, "link", link))
            count += 2

    available, arrived, done = {}, {}, {}
    while events:
        now, _, kind, name = heapq.heappop(events)
        if kind == "link":
            serve(name, now)
        elif kind == "free":
            done[name] = now
            for message in leaving[name]:
                task, link, size, rank = messages[message]
                available[message] = now
                heapq.heappush(queue[link], ((99, now) if rank is None else rank, count, message))
                count += 1
                serve(link, now)
        targets = [name] if kind == "part" else users[name] if kind in ("arrive", "free") else []
        if kind == "arrive":
            arrived[name] = now
        for task in targets:
            left[task] -= 1
            if left[task] == 0:
                heapq.heappush(ready, (tasks[task][2], count, task))
                count += 1
        while ready and core_free <= now + 1e-9:
            if events and events[0][0] <= now + 1e-9 and events[0][2] != "link":
                break
            task = heapq.heappop(ready)[-1]
            items.append((now, 0, len(items), "task", task))
            core_free = now + tasks[task][1]
            heapq.heappush(events, (core_free, count, "free", task))
            count += 1
    assert len(done) == len(tasks), "cycle"
    items.sort()
    sent = set()
    for _, _, _, kind, name in items:
        if kind == "send":
            sent.add(name)
        else:
            assert all(n in done or n in sent for n in tasks[name][0]), "order"
            sent.update(m for m in leaving[name] if messages[m][3] is None)
    return items, done


def turned_dot(left, right):
    return lax.dot_general(left, right, (((1,), (1,)), ((), ())), preferred_element_type=F32)


def layer_kernel(
    tokens, mix_gain, query_w, key_w, value_w, head_gain, out_w, chan_gain, up_w, down_w, cosine, sine,
    result,
    w_both, w_value, w_out, w_up, w_down, down_turned,
    blocks, normed, middle, mix_row, chan_row, head_rows, cos_tab, sin_tab, decay,
    raw, raw_value, query, keys, values, head_out, hidden,
    terms1, give1, take1, move1, left1, right1, pass1,
    terms2, give2, take2, move2, left2, right2, pass2,
    local_sem, send_sem, recv_sem,
):
    rep, fs, tp = lax.axis_index("rep"), lax.axis_index("fs"), lax.axis_index("tp")
    z, y = fs // NY, fs % NY
    x, core = tp // 2, tp % 2
    units = (w_both, w_value, w_out, w_up, w_down)
    target = {
        ("y", 1): {"fs": z * NY + (y + 1) % NY},
        ("y", -1): {"fs": z * NY + (y + NY - 1) % NY},
        ("z", 1): {"rep": (rep + (z + 1) // NZ) % 2, "fs": ((z + 1) % NZ) * NY + y},
        ("z", -1): {"rep": (rep + (NZ - z) // NZ) % 2, "fs": ((z + NZ - 1) % NZ) * NY + y},
        ("x", 1): {"tp": ((x + 1) % NX) * 2 + core},
        ("x", -1): {"tp": ((x + NX - 1) % NX) * 2 + core},
        "partner": {"tp": x * 2 + (1 - core)},
    }
    barrier = pltpu.get_barrier_semaphore()
    for k in target:
        pl.semaphore_signal(barrier, inc=1, device_id=target[k], device_id_type=MESH)

    def slot(a, b):
        at = ((z - b + NZ) % NZ) * NY + (y - a + NY) % NY
        return pl.ds(pl.multiple_of(at * 64, 64), 64)

    mine = slot(0, 0)
    local = []

    def bring(source, dest):
        copy = pltpu.make_async_copy(source, dest, local_sem.at[len(local)])
        copy.start()
        local.append(copy)

    bring(tokens, blocks.at[tp])
    bring(query_w, w_both.at[mine, 0:DK])
    bring(key_w, w_both.at[mine, DK : 2 * DK])
    bring(value_w, w_value.at[mine])
    bring(out_w, w_out.at[mine])
    bring(up_w, w_up.at[mine])
    bring(down_w, w_down.at[mine])
    bring(mix_gain, mix_row)
    bring(chan_gain, chan_row)
    bring(head_gain, head_rows)
    bring(cosine, cos_tab)
    bring(sine, sin_tab)
    for copy in local[:4]:
        copy.wait()
    pl.semaphore_wait(barrier, len(target))

    tasks, bodies = {}, {}
    messages, views = {}, {}
    lands, leaves, totals = {}, {}, {}

    def task(name, needs, cost, rank, body=None, start=0.0):
        tasks[name] = (needs, cost, rank, start)
        bodies[name] = body

    def message(name, after, link, size, source, dest, here, rank=None, share=None, sent=None):
        messages[name] = (after, link, size, rank)
        views[name] = (source, dest, share[1] if share else here)
        lands[name] = share[0] if share else name
        leaves[name] = sent[0]
        totals[sent[0]] = sent[1]

    def piece(p, a, b):
        u, first, count = PARTS[p][:3]
        at = ((z - b + NZ) % NZ) * NY + (y - a + NY) % NY
        return units[u].at[pl.ds(pl.multiple_of(at * 64 + first, 16), count)]

    inside = defaultdict(list)
    for p, (u, _, count, _, rank, start) in enumerate(PARTS):
        stack, ends = [(0, 0)], defaultdict(list)
        sent = (("w", p), units[u].at[pl.ds(0, 31 * count)])
        seen = {}
        while stack:
            a, b = stack.pop()
            seen[a, b] = onward(p, a, b)
            if not seen[a, b]:
                ends[2 if abs(b) == 2 else b].append((a, b))
            stack += [(na, nb) for _, na, nb in seen[a, b]]
        for (a, b), following in seen.items():
            if not following:
                continue
            name = ("w", p, a, b)
            needs = ([] if u < 2 else ["prepare"]) if (a, b) == (0, 0) else [name]
            task(("got", *name), needs, 0.02, -1, None, start)
            inside[u].append(("got", *name))
            for k, na, nb in following:
                group = [(g, e) for g, e in ends.items() if (na, nb) in e]
                share = None
                if group:
                    share = (("end", p, group[0][0]), units[u].at[pl.ds(0, len(group[0][1]) * count)])
                message(
                    ("w", p, na, nb), ("got", *name), k, count * 1024,
                    piece(p, a, b), piece(p, a, b), piece(p, na, nb), (rank, -1 - below(p, na, nb)), share, sent,
                )
        for g, group in ends.items():
            name = ("got", "w", p, "end", g)
            task(name, [("w", p, a, b) for a, b in group], 0.02, 1, None)
            inside[u].append(name)

    planes = (0, 1, -1, 2)

    def plane(b):
        return (z - b + NZ) % NZ

    def of_plane(u, b):
        return [n for n in inside[u] if n[-1] in ((2, -2) if b == 2 else (b,))]

    def plane_rows(b):
        return pl.ds(pl.multiple_of(plane(b) * 512, 512), 512)

    def turn(b):
        at = pl.multiple_of(plane(b) * 512, 512)
        for n in range(4):
            down_turned[:, pl.ds(at + n * 128, 128)] = w_down[pl.ds(at + n * 128, 128), :].T

    for b in planes:
        task(("turn", b), of_plane(4, b), 0.22, 2, lambda b=b: turn(b))
    turned = [("turn", b) for b in planes]

    def at_x(o):
        return (x + o + NX) % NX

    def gather(tag, view, size, first, needs, rank, ref, sent):
        task((tag, 0, 0), needs, 0.01 if first is None else first[0], 0, first and first[1])
        parts = [(0, 0), (-1, 0), (1, 1), (-1, 1), (1, 0), (-2, 0), (2, 1)]
        for o, h in parts[1:]:
            task((tag, o, h), [(tag, "m", o, h)], 0.02, 0)
        task((tag, "p"), [(tag, "mp", o, h) for o, h in parts + [(0, 1)]], 0.02, 1)

        def pass_on(o, h, after, link, no):
            message((tag, "m", no, h), after, link, size, view(o, core, h), view(o, core, h), view(no, core, h), (*rank, 0 if no in (-2, 2) else 1), None, sent)

        pass_on(0, 0, (tag, 0, 0), ("x", 1), -1)
        pass_on(0, 1, (tag, 0, 0), ("x", -1), 1)
        pass_on(0, 1, (tag, 0, 0), ("x", 1), -1)
        pass_on(0, 0, (tag, 0, 0), ("x", -1), 1)
        pass_on(-1, 0, (tag, -1, 0), ("x", 1), -2)
        pass_on(1, 1, (tag, 1, 1), ("x", -1), 2)
        for o, h in parts + [(0, 1)]:
            after = (tag, 0, 0) if o == 0 else (tag, o, h)
            message(
                (tag, "mp", o, h), after, "partner", size,
                view(o, core, h), view(o, core, h), view(o, 1 - core, h), None, ((tag, "p"), ref), sent,
            )
        return [(tag, o, h) for o, h in parts] + [(tag, "p")]

    def token_view(o, c, h):
        return blocks.at[at_x(o) * 2 + c, pl.ds(h * 256, 256)]

    all_tokens = gather("t", token_view, 131072, None, [], (0, 0), blocks.at[pl.ds(0, 4)], ("t", blocks.at[pl.ds(0, 7)]))

    def prepare():
        for copy in local[4:]:
            copy.wait()
        rate = jnp.float32(0.0)
        for h in range(8):
            rate = jnp.where(tp == h, jnp.float32(np.log1p(-(2.0 ** (-5 - h)))), rate)
        offset = (
            lax.broadcasted_iota(jnp.int32, (128, 128), 0) - lax.broadcasted_iota(jnp.int32, (128, 128), 1)
        ).astype(F32)
        for n in range(4):
            value = jnp.exp(rate * jnp.maximum(offset + 128.0 * n, 0.0))
            decay[n] = jnp.where(offset + 128.0 * n >= 0, value, 0.0)

    task("prepare", [], 0.4, -2, prepare, 0.5)

    def scaled(dest, read, gain, rows):
        total = jnp.zeros((64, 256), F32)
        for b in range(8):
            part = read(b, rows).astype(F32)
            total = total + part * part
        scale = lax.rsqrt(jnp.sum(total, axis=-1, keepdims=True) * (1.0 / D) + EPS)
        for b in range(8):
            columns = slice(b * 256, (b + 1) * 256)
            dest[rows, columns] = (read(b, rows).astype(F32) * scale * gain[:, columns]).astype(BF)

    def norm_tokens(n):
        @pl.loop(0, 4)
        def _(i):
            rows = pl.ds(pl.multiple_of(n * 256 + i * 64, 64), 64)
            scaled(normed, lambda b, r: blocks[b, r, :], mix_row, rows)

    for n in range(2):
        task(("norm", n), all_tokens + ["prepare"], 0.65, 2, lambda n=n: norm_tokens(n))

    def columns_of(n):
        return slice(n * 256, (n + 1) * 256)

    def project(weights, dest, b):
        at = plane_rows(b)

        @pl.loop(0, 2)
        def _(n):
            columns = pl.ds(pl.multiple_of(n * 256, 256), 256)
            value = jnp.dot(normed[:, at], weights[at, columns], preferred_element_type=F32)
            dest[:, columns] = value if b == 0 else dest[:, columns] + value

    def round_values():
        values[...] = raw_value[...].astype(BF)

    def rotary():
        @pl.loop(0, ROWS // 64)
        def _(i):
            rows = pl.ds(pl.multiple_of(i * 64, 64), 64)
            c, s = cos_tab[rows, :], sin_tab[rows, :]
            for start, dest, factor in ((0, query, 1.0), (DK, keys, DK**-0.5)):
                first, second = raw[rows, start : start + 128], raw[rows, start + 128 : start + 256]
                dest[rows, 0:128] = ((first * c - second * s) * factor).astype(BF)
                dest[rows, 128:256] = ((second * c + first * s) * factor).astype(BF)

    before = [("norm", 0), ("norm", 1)]
    for u, dest, name in ((0, raw, "both"), (1, raw_value, "value")):
        last = []
        for b in planes:
            task(
                (name, b), of_plane(u, b) + before + last, 0.6, 3,
                lambda u=u, dest=dest, b=b: project(units[u], dest, b),
            )
            last = [(name, b)]
    task("rotary", [("both", 2)], 0.25, 3, rotary)
    task("values", [("value", 2)], 0.1, 3, round_values)

    def retain(i):
        gain = head_rows[pl.ds(tp, 1), :]
        rows = slice(i * 128, (i + 1) * 128)
        total = jnp.zeros((128, DV), F32)
        for j in range(i + 1):
            there = slice(j * 128, (j + 1) * 128)
            score = turned_dot(query[rows, :], keys[there, :]) * decay[i - j]
            total = total + jnp.dot(score.astype(BF), values[there, :], preferred_element_type=F32)
        scale = lax.rsqrt(jnp.mean(total * total, axis=-1, keepdims=True) + HEAD_EPS)
        head_out[rows, :] = (total * scale * gain).astype(BF)

    for i in range(4):
        task(("retain", i), ["rotary", "values"], 0.4 + 0.1 * i, 3, lambda i=i: retain(i))

    def reduce(tag, i, needs, cost, compute, buffers, part, half, size, settle, settle_cost):
        give, take, move, left, right, through = buffers
        task((tag, "terms", i), needs, cost, 3 + i, compute)
        message(
            (tag, "give", i), (tag, "terms", i), "partner", 8 * size, give.at[i], take.at[i], take.at[i],
            None, None, ((tag, "give"), give),
        )

        def spread():
            for n, (o, h) in enumerate(((2, 0), (2, 1), (1, 1), (-1, 0))):
                move[i, n] = part(i, o, h).astype(BF)

        task((tag, "spread", i), [(tag, "give", i)], 0.1, 1, spread)
        for n, (link, dest) in enumerate(
            (
                (("x", 1), through.at[i, 0]),
                (("x", -1), through.at[i, 1]),
                (("x", 1), left.at[(i, *half(1))]),
                (("x", -1), right.at[(i, *half(0))]),
                (("x", 1), left.at[(i, *half(0))]),
                (("x", -1), right.at[(i, *half(1))]),
            )
        ):
            after = (tag, "spread", i) if n < 4 else (tag, "merge", i, n - 4)
            message((tag, "move", i, n), after, link, size, move.at[i, n], dest, dest, (*XRANK[tag, i], (1, 1, 2, 2, 0, 0)[n]),
                None if n < 2 else ((tag, "last", i), move.at[i, pl.ds(0, 4)]), ((tag, "move"), move))

        def merge(h):
            o = 1 if h == 0 else -1
            move[i, 4 + h] = (part(i, o, h) + through[i, h].astype(F32)).astype(BF)

        for h in range(2):
            task(
                (tag, "merge", i, h), [(tag, "move", i, h), (tag, "spread", i)], 0.06, 0, lambda h=h: merge(h)
            )
        needs = [(tag, "spread", i)] + [(tag, "move", i, n) for n in range(2, 6)]
        return needs, settle_cost, settle

    def half1(h):
        return (slice(h * 32, (h + 1) * 32), slice(None))

    def part1(i, o, h):
        rows, columns = half1(h)
        return terms1[i, core, at_x(o), rows, columns] + take1[i, at_x(o), rows, columns].astype(F32)

    def out_terms(i):
        at = pl.multiple_of(plane(planes[i]) * 512, 512)
        for n in range(2):
            value = turned_dot(head_out[...], w_out[pl.ds(at + n * 256, 256), :])
            terms1[i, :, :, :, columns_of(n)] = value.reshape(2, 4, 64, 256)
        give1[i] = terms1[i, 1 - core].astype(BF)

    def token_rows(o, c, h=None):
        start, size = (0, 64) if h is None else (h * 32, 32)
        return pl.ds(pl.multiple_of(c * 256 + at_x(o) * 64 + start, size), size)

    def settle1(i):
        p = plane(planes[i])
        rows = token_rows(0, core)
        total = terms1[i, core, x] + take1[i, x].astype(F32) + left1[i].astype(F32) + right1[i].astype(F32)
        for n in range(2):
            middle[p, rows, columns_of(n)] = (total[:, columns_of(n)] + blocks[2 * p + n, rows, :].astype(F32)).astype(BF)

    def middle_view(i):
        return lambda o, c, h: middle.at[plane(planes[i]), token_rows(o, c, h)]

    def norm_middle(i):
        @pl.loop(0, 2)
        def _(n):
            rows = pl.ds(pl.multiple_of(i * 128 + n * 64, 64), 64)
            scaled(normed, lambda b, r: middle[b // 2, r, columns_of(b % 2)], chan_row, rows)

    def mix_up(i):
        rows = slice(i * 128, (i + 1) * 128)
        for n in range(2):
            value = jnp.maximum(
                jnp.dot(normed[rows, :], w_up[:, columns_of(n)], preferred_element_type=F32), 0.0
            )
            hidden[rows, columns_of(n)] = (value * value).astype(BF)

    def half2(h):
        return (slice(h * 64, (h + 1) * 64), slice(None))

    def part2(i, o, h):
        rows, columns = half2(h)
        return terms2[i, at_x(o), core, rows, columns] + take2[i, at_x(o), rows, columns].astype(F32)

    def down_terms(i):
        rows = slice(i * 128, (i + 1) * 128)

        for n in range(8):
            value = jnp.dot(hidden[rows, :], down_turned[:, columns_of(n)], preferred_element_type=F32)
            terms2[i, n // 2, n % 2] = value

        for n in range(4):
            give2[i, n] = terms2[i, n, 1 - core].astype(BF)

    def settle2(i):
        rows = slice(i * 128, (i + 1) * 128)
        total = terms2[i, x, core] + take2[i, x].astype(F32)
        total = total + left2[i].astype(F32) + right2[i].astype(F32)
        columns = pl.ds(pl.multiple_of(core * 256, 256), 256)
        result[rows, :] = total + middle[x, rows, columns].astype(F32)

    pieces = []
    for i, b in enumerate(planes):
        needs, cost, body = reduce(
            "m", i, of_plane(2, b) + [("retain", n) for n in range(4)], 0.5, lambda i=i: out_terms(i),
            (give1, take1, move1, left1, right1, pass1), part1, half1, 32768, lambda i=i: settle1(i), 0.08,
        )
        pieces += gather(
            ("c", i), middle_view(i), 32768, (cost, body), needs, XRANK["c", i],
            middle.at[0, pl.ds(0, 256)], ("c", middle.at[:, pl.ds(0, 448)]),
        )
    for i in range(4):
        task(("norm2", i), pieces + [("both", 2), ("value", 2)], 0.32, 3 + i, lambda i=i: norm_middle(i))
        task(("up", i), inside[3] + [("norm2", i)], 0.45, 3 + i, lambda i=i: mix_up(i))
        needs, cost, body = reduce(
            "d", i, turned + [("up", i)], 0.52, lambda i=i: down_terms(i),
            (give2, take2, move2, left2, right2, pass2), part2, half2, 32768, lambda i=i: settle2(i), 0.08,
        )
        task(("last", i), needs, cost, 1, body)

    items, _ = schedule(tasks, messages)
    number = {n: k for k, n in enumerate(dict.fromkeys(lands.values()))}
    sender = {n: k for k, n in enumerate(totals)}
    assert len(number) <= LANDS and len(sender) <= SENDS, "semaphores"

    def start(name):
        source, dest, _ = views[name]
        copy = pltpu.make_async_remote_copy(
            src_ref=source,
            dst_ref=dest,
            send_sem=send_sem.at[sender[leaves[name]]],
            recv_sem=recv_sem.at[number[lands[name]]],
            device_id=target[messages[name][1]],
            device_id_type=MESH,
        )
        copy.start()

    departing = defaultdict(list)
    for name, (after, _, _, rank) in messages.items():
        if rank is None:
            departing[after].append(name)
    for _, _, _, kind, name in items:
        if kind == "send":
            start(name)
            continue
        waits = [n for n in tasks[name][0] if n in messages]
        if waits:
            for key in dict.fromkeys(lands[n] for n in waits):
                here = next(views[n][2] for n in waits if lands[n] == key)
                pltpu.make_async_copy(here, here, recv_sem.at[number[key]]).wait()
        if bodies[name]:
            bodies[name]()
        for n in departing[name]:
            start(n)
    for key, whole in totals.items():
        pltpu.make_async_copy(whole, whole, send_sem.at[sender[key]]).wait()


def rotary_tables():
    half = DK // 2
    angle = np.arange(ROWS)[:, None] * THETA ** (-np.arange(half) / half)
    return np.cos(angle).astype(np.float32), np.sin(angle).astype(np.float32)


def shards(tokens, mix_gain, query_w, key_w, value_w, head_gain, out_w, chan_gain, up_w, down_w):
    cosine, sine = rotary_tables()
    any_place = pl.BlockSpec(memory_space=pl.ANY)
    vmem = pltpu.VMEM
    scratch = [
        *[vmem((D, 512), BF)] * 5,
        vmem((512, D), BF),
        vmem((8, ROWS, 256), BF),
        vmem((ROWS, D), BF),
        vmem((4, ROWS, 512), BF),
        vmem((1, D), F32),
        vmem((1, D), F32),
        vmem((8, DV), F32),
        vmem((ROWS, DK // 2), F32),
        vmem((ROWS, DK // 2), F32),
        vmem((4, 128, 128), F32),
        vmem((ROWS, 512), F32),
        vmem((ROWS, 512), F32),
        vmem((ROWS, DK), BF),
        vmem((ROWS, DK), BF),
        vmem((ROWS, DV), BF),
        vmem((ROWS, DV), BF),
        vmem((ROWS, 512), BF),
        vmem((4, 2, 4, 64, 512), F32),
        vmem((4, 4, 64, 512), BF),
        vmem((4, 4, 64, 512), BF),
        vmem((4, 6, 32, 512), BF),
        vmem((4, 64, 512), BF),
        vmem((4, 64, 512), BF),
        vmem((4, 2, 32, 512), BF),
        vmem((4, 4, 2, 128, 256), F32),
        vmem((4, 4, 128, 256), BF),
        vmem((4, 4, 128, 256), BF),
        vmem((4, 6, 64, 256), BF),
        vmem((4, 128, 256), BF),
        vmem((4, 128, 256), BF),
        vmem((4, 2, 64, 256), BF),
        pltpu.SemaphoreType.DMA((12,)),
        pltpu.SemaphoreType.DMA((SENDS,)),
        pltpu.SemaphoreType.DMA((LANDS,)),
    ]
    whole = pl.pallas_call(
        layer_kernel,
        out_shape=jax.ShapeDtypeStruct((ROWS, 256), F32),
        in_specs=[any_place] * 12,
        out_specs=pl.BlockSpec(memory_space=pltpu.VMEM),
        scratch_shapes=scratch,
        compiler_params=pltpu.CompilerParams(
            collective_id=0, has_side_effects=True, vmem_limit_bytes=60 << 20
        ),
        name="layer",
    )(
        tokens, mix_gain.reshape(1, D), query_w, key_w, value_w, head_gain, out_w.T,
        chan_gain.reshape(1, D), up_w, down_w.T, jnp.asarray(cosine), jnp.asarray(sine),
    )
    return whole.astype(BF)


def solution(mesh):
    placed = (
        P(("rep", "fs"), "tp"),
        P(),
        P("fs", "tp"),
        P("fs", "tp"),
        P("fs", "tp"),
        P(),
        P("tp", "fs"),
        P(),
        P("fs", "tp"),
        P("tp", "fs"),
    )
    return jax.shard_map(
        shards, mesh=mesh, in_specs=placed, out_specs=P(("rep", "fs"), "tp"), check_vma=False
    )
```

time: 314 us -> 99.7 us (0.32)
  waiting for transfers between devices: 143 us -> 0 us
  blocking collectives: 109 us -> 0 us
  Pallas kernels: 0 us -> 97.3 us
  matrix products: 19.2 us -> 0 us
  between operations: 13.7 us -> 0.01 us
  starting transfers between devices: 10.3 us -> 0 us
  local copies, waits for them, and re-layouts: 9.88 us -> 0 us
  other arithmetic: 7.86 us -> 1.77 us
    all_gather x1 -> x0, waiting for transfers between devices: 117 us -> none  [gather_turned(): lax.all_gather(both, axis, axis=0, tiled=True)]
    all_to_all x3 -> x0, blocking collectives: 109 us -> none  [the longest x2 78.9 us: sum_at_owner(): lax.all_to_all(cut_along(value, dim, count), axis, 0, 0, tiled=True)]
    pallas_call x0 -> x1, Pallas kernels: none -> 97.3 us  [shards(): pl.pallas_call(layer_kernel, out_shape=jax.ShapeDtypeStruct((ROWS, 256),...]
    all_to_all x1 -> x0, waiting for transfers between devices: 26.1 us -> none  [copy_for_each(): lax.all_to_all(jnp.broadcast_to(value[None], (count, *value.shape)), axis...]
    dot_general x17 -> x0, matrix products: 19.2 us -> none  [the longest x1 5.23 us: shards(): chan_terms = jnp.dot(hidden, down_all, preferred_element_type=jnp.float32)]
    all_to_all x1 -> x0, starting transfers between devices: 10.3 us -> none  [copy_for_each(): lax.all_to_all(jnp.broadcast_to(value[None], (count, *value.shape)), axis...]
    unnamed x22 -> x0, local copies, waits for them, and re-layouts: 6.96 us -> none
  transfers between devices with their start and end apart: 2 -> 0, of which waited for: 2 -> 0; matrix products, arithmetic and copies ran while one was open for 2% -> 0% of each run, Pallas kernels for 0% -> 0%
where the time goes in v3:
time: 99.7 us; the launch traced here: 99.1 us
  Pallas kernels  97.3 us (98%)
  other arithmetic  1.77 us (2%)
    pallas_call x1, Pallas kernels, shards(): pl.pallas_call(layer_kernel, out_shape=jax.ShapeDtypeStruct((ROWS, 256),...  97.3 us

profile of v3, /device:TPU:1, one launch (start us, length us, event | category | flops | bytes accessed | tf_op | source)
XLA Modules:
  0.0 99.1 jit_solution(15498667364166688035)
XLA Ops:
  0.0 97.3 %layer.1 = f32[512,256]{1,0:T(8,128)} custom-call(bf16[512,256]{1,0:T(8,128)(2,1)} %tokens.1, f32[1,2048]{1,0:T(1,128)} %bitcast.6, bf16[64,256]{1,0:T(8,128)(2,1)} %query_w.1, bf16[64,256]{1,0:T(8,128)(2,1)} %key_w.1, bf16[64,512]{1,0:T(8,128)(2,1)} %value_w.1, f32[8,512]{1,0:T(8,128)} %head_gain.1, bf16[64,512]{1,0:T(8,128)(2,1)} %bitcast.4, ...), custom_call_target="tpu_custom_call" | custom-call | tf_op jit(solution)/shard_map/layer/pallas_call | solution.py:600
  97.3 1.8 %convert_element_type.3 = bf16[512,256]{1,0:T(8,128)(2,1)} convert(f32[512,256]{1,0:T(8,128)} %layer.1) | non-fusion elementwise | flops 131072 | bytes 786432 | tf_op jit(solution)/shard_map/convert_element_type | solution.py:614

commit v4 on v3

--- a/solution.py
+++ b/solution.py
@@ -30,10 +30,10 @@
     (4, 32, 32, "B", 2, 2.5),
 )
 SENDS, LANDS = 13, 220
-LEAD = {"y": 3.2, "z": 3.2, "x": 2.0}
+LEAD = {"y": 1.5, "z": 1.5, "x": 1.2}
 XRANK = {(t, i): (i + 1.5 * k, k) for k, t in enumerate("mcd") for i in range(4)}
 RATE = {"ring": 45.2e3, "partner": 600e3}
-DELAY = {"early": 2.3, "late": 3.0, "x": 2.2, "partner": 1.1}
+DELAY = {"early": 2.3, "late": 2.5, "x": 2.2, "partner": 1.1}
 
 
 def onward(p, a, b):
@@ -153,7 +153,7 @@
     raw, raw_value, query, keys, values, head_out, hidden,
     terms1, give1, take1, move1, left1, right1, pass1,
     terms2, give2, take2, move2, left2, right2, pass2,
-    local_sem, send_sem, recv_sem,
+    answer, local_sem, send_sem, recv_sem,
 ):
     rep, fs, tp = lax.axis_index("rep"), lax.axis_index("fs"), lax.axis_index("tp")
     z, y = fs // NY, fs % NY
@@ -491,7 +491,8 @@
         total = terms2[i, x, core] + take2[i, x].astype(F32)
         total = total + left2[i].astype(F32) + right2[i].astype(F32)
         columns = pl.ds(pl.multiple_of(core * 256, 256), 256)
-        result[rows, :] = total + middle[x, rows, columns].astype(F32)
+        answer[rows, :] = (total + middle[x, rows, columns].astype(F32)).astype(BF)
+        pltpu.make_async_copy(answer.at[rows], result.at[rows], local_sem.at[i]).start()
 
     pieces = []
     for i, b in enumerate(planes):
@@ -546,6 +547,9 @@
             bodies[name]()
         for n in departing[name]:
             start(n)
+    for i in range(4):
+        rows = slice(i * 128, (i + 1) * 128)
+        pltpu.make_async_copy(answer.at[rows], result.at[rows], local_sem.at[i]).wait()
     for key, whole in totals.items():
         pltpu.make_async_copy(whole, whole, send_sem.at[sender[key]]).wait()
 
@@ -593,15 +597,16 @@
         vmem((4, 128, 256), BF),
         vmem((4, 128, 256), BF),
         vmem((4, 2, 64, 256), BF),
+        vmem((ROWS, 256), BF),
         pltpu.SemaphoreType.DMA((12,)),
         pltpu.SemaphoreType.DMA((SENDS,)),
         pltpu.SemaphoreType.DMA((LANDS,)),
     ]
     whole = pl.pallas_call(
         layer_kernel,
-        out_shape=jax.ShapeDtypeStruct((ROWS, 256), F32),
+        out_shape=jax.ShapeDtypeStruct((ROWS, 256), BF),
         in_specs=[any_place] * 12,
-        out_specs=pl.BlockSpec(memory_space=pltpu.VMEM),
+        out_specs=any_place,
         scratch_shapes=scratch,
         compiler_params=pltpu.CompilerParams(
             collective_id=0, has_side_effects=True, vmem_limit_bytes=60 << 20
@@ -611,7 +616,7 @@
         tokens, mix_gain.reshape(1, D), query_w, key_w, value_w, head_gain, out_w.T,
         chan_gain.reshape(1, D), up_w, down_w.T, jnp.asarray(cosine), jnp.asarray(sine),
     )
-    return whole.astype(BF)
+    return whole
 
 
 def solution(mesh):

time: 99.7 us -> 96.8 us (0.971)
  Pallas kernels: 97.3 us -> 94.9 us
  other arithmetic: 1.77 us -> 0 us
  local copies, waits for them, and re-layouts: 0 us -> 1.67 us
    pallas_call x1, Pallas kernels: 97.3 us -> 94.9 us  [shards(): pl.pallas_call(layer_kernel, out_shape=jax.ShapeDtypeStruct((ROWS, 256),...]
    convert_element_type x1 -> x0, other arithmetic: 1.77 us -> none  [shards(): return whole.astype(BF)]
    unnamed x0 -> x1, local copies, waits for them, and re-layouts: none -> 1.67 us
where the time goes in v4:
time: 96.8 us; the launch traced here: 96.6 us
  Pallas kernels  94.9 us (98%)
  local copies, waits for them, and re-layouts  1.67 us (2%)
    pallas_call x1, Pallas kernels, shards(): pl.pallas_call(layer_kernel, out_shape=jax.ShapeDtypeStruct((ROWS, 256),...  94.9 us

profile of v4, /device:TPU:1, one launch (start us, length us, event | category | flops | bytes accessed | tf_op | source)
XLA Modules:
  0.0 96.6 jit_solution(13598760534288999949)
XLA Ops:
  0.0 94.9 %layer.1 = bf16[512,256]{1,0:T(8,128)(2,1)} custom-call(bf16[512,256]{1,0:T(8,128)(2,1)} %tokens.1, f32[1,2048]{1,0:T(1,128)} %bitcast.6, bf16[64,256]{1,0:T(8,128)(2,1)} %query_w.1, bf16[64,256]{1,0:T(8,128)(2,1)} %key_w.1, bf16[64,512]{1,0:T(8,128)(2,1)} %value_w.1, f32[8,512]{1,0:T(8,128)} %head_gain.1, bf16[64,512]{1,0:T(8,128)(2,1)} %bitcast.4, ...), custom_call_target="tpu_custom_call" | custom-call | tf_op jit(solution)/shard_map/layer/pallas_call | solution.py:605
  94.9 1.7 %copy.14 = bf16[512,256]{1,0:T(8,128)(2,1)} copy(bf16[512,256]{1,0:T(8,128)(2,1)} %layer.1) | data formatting | bytes 524288

commit v5 on v4

--- a/solution.py
+++ b/solution.py
@@ -23,13 +23,11 @@
 PARTS = (
     (0, 0, 64, "A", 0, 0.0),
     (1, 0, 64, "B", 1, 0.0),
-    (2, 0, 64, "A", 1, 1.0),
-    (3, 0, 32, "A", 2, 2.5),
-    (3, 32, 32, "B", 2, 2.5),
-    (4, 0, 32, "A", 2, 2.5),
-    (4, 32, 32, "B", 2, 2.5),
+    (2, 0, 64, "A", 1, 1.5),
+    (3, 0, 64, "B", 2, 2.5),
+    (4, 0, 64, "A", 2, 2.5),
 )
-SENDS, LANDS = 13, 220
+SENDS, LANDS = 11, 175
 LEAD = {"y": 1.5, "z": 1.5, "x": 1.2}
 XRANK = {(t, i): (i + 1.5 * k, k) for k, t in enumerate("mcd") for i in range(4)}
 RATE = {"ring": 45.2e3, "partner": 600e3}

time: 96.8 us -> 96.1 us (level)
  no operation moved by 1% of the time
where the time goes in v5:
time: 96.1 us; the launch traced here: 95.9 us
  Pallas kernels  94.2 us (98%)
  local copies, waits for them, and re-layouts  1.67 us (2%)
    pallas_call x1, Pallas kernels, shards(): pl.pallas_call(layer_kernel, out_shape=jax.ShapeDtypeStruct((ROWS, 256),...  94.2 us

profile of v5, /device:TPU:1, one launch (start us, length us, event | category | flops | bytes accessed | tf_op | source)
XLA Modules:
  0.0 95.9 jit_solution(13535886808914634343)
XLA Ops:
  0.0 94.2 %layer.1 = bf16[512,256]{1,0:T(8,128)(2,1)} custom-call(bf16[512,256]{1,0:T(8,128)(2,1)} %tokens.1, f32[1,2048]{1,0:T(1,128)} %bitcast.6, bf16[64,256]{1,0:T(8,128)(2,1)} %query_w.1, bf16[64,256]{1,0:T(8,128)(2,1)} %key_w.1, bf16[64,512]{1,0:T(8,128)(2,1)} %value_w.1, f32[8,512]{1,0:T(8,128)} %head_gain.1, bf16[64,512]{1,0:T(8,128)(2,1)} %bitcast.4, ...), custom_call_target="tpu_custom_call" | custom-call | tf_op jit(solution)/shard_map/layer/pallas_call | solution.py:603
  94.3 1.7 %copy.14 = bf16[512,256]{1,0:T(8,128)(2,1)} copy(bf16[512,256]{1,0:T(8,128)(2,1)} %layer.1) | data formatting | bytes 524288
